TPU v7x, 32 devices: a whole 2x2x4 slice. The times are simulated.
32 devices in a mesh: sp: 8 (over z, x), tp: 4 (over y, core).
Axes of the slice: x: 2, y: 2, z: 4, core: 2. Of those that a mesh axis runs over, the one named last changes fastest.
Arguments:
- sequence_activations: bfloat16 [4096, 2048], P('sp', 'tp'), may hold values from -45 to 45
- entry_rescale_vector: float32 [2048], replicated, may hold values from 0.1 to 1.9
- blender_exit_switch_matrix: bfloat16 [2048, 2048], P('sp', 'tp'), may hold values from -0.125 to 0.125
- blender_entry_switch_matrix: bfloat16 [2048, 2048], P('sp', 'tp'), may hold values from -0.125 to 0.125
- blender_payload_matrix: bfloat16 [2048, 2048], P('sp', 'tp'), may hold values from -0.125 to 0.125
- scan_entry_matrix: bfloat16 [2048, 2048], P('sp', 'tp'), may hold values from -0.125 to 0.125
- scan_exit_switch_matrix: bfloat16 [2048, 2048], P('sp', 'tp'), may hold values from -0.125 to 0.125
- filter_blend_matrix: bfloat16 [2048, 2048], P('sp', 'tp'), may hold values from -0.125 to 0.125
- scan_blend_matrix: bfloat16 [2048, 2048], P('sp', 'tp'), may hold values from -0.125 to 0.125
- blender_kernel_coefficients: bfloat16 [3, 2048], P(None, 'tp'), may hold values from -3.5 to 3.5
- scan_kernel_coefficients: bfloat16 [4, 2048], P(None, 'tp'), may hold values from -3 to 3
- scan_switch_blockwise: bfloat16 [8, 256, 256], P('tp'), may hold values from -0.375 to 0.375
- entry_switch_blockwise: bfloat16 [8, 256, 256], P('tp'), may hold values from -0.375 to 0.375
- feature_fade_odds: float32 [2048], P('tp'), may hold values from 3 to 16
- fade_speed_multiplier: float32 [4096], P('sp'), may hold values from 0.3 to 2.8
- added_rate_shift: float32 [4096], P('sp'), may hold values from -1.4 to 0
- initial_hidden_vector: float32 [2048], P('tp'), may hold values from -6 to 6
- filter_exit_matrix: bfloat16 [2048, 2048], P('tp'), may hold values from -0.125 to 0.125
- scan_exit_matrix: bfloat16 [2048, 2048], P('tp'), may hold values from -0.125 to 0.125
Outputs:
- mixed: bfloat16 [4096, 2048], P('sp', 'tp')
All inputs are finite; a program needn't handle non-finite values.
Results may differ from a plain program's by a relative error of at most 0.015.
Values may be sent and summed in bfloat16 or wider, within the bound.
A program may use at most 64 MiB of HBM per device.

v0:
```python
import jax
import jax.numpy as jnp
from jax import lax
from jax.sharding import PartitionSpec as P

scan_switch_exponent = 8.0
norm_eps = 1e-06


def passed_along(value, axis, by):
    peers = lax.axis_size(axis)
    pairs = [(i, i + by) for i in range(peers) if 0 <= i + by < peers]
    return lax.ppermute(value, axis, pairs)


def entering(value, axis, combine, identity):
    peers, place = (lax.axis_size(axis), lax.axis_index(axis))
    everything = jax.tree.map(lambda part: lax.all_gather(part, axis), value)
    start = jax.tree.map(
        lambda part, zero: jnp.broadcast_to(jnp.asarray(zero, part.dtype), part.shape),
        value,
        identity,
    )

    def step(k, before):
        reached = k < place
        new = combine(before, jax.tree.map(lambda part: part[k], everything))
        return jax.tree.map(lambda a, b: jnp.where(reached, a, b), new, before)

    return lax.fori_loop(0, peers, step, start)


def linear_chain(earlier, later):
    return (earlier[0] * later[0], later[0] * earlier[1] + later[1])


def causal_local(previous, values, weights):
    taps = weights.shape[0]
    length = values.shape[0]
    extended = jnp.concatenate([previous, values], axis=0)
    result = extended[0:length] * weights[0].astype(jnp.float32)
    for tap_index in range(1, taps):
        result = result + extended[tap_index : tap_index + length] * weights[tap_index].astype(
            jnp.float32
        )
    return result


def local(
    sequence_activations,
    entry_rescale_vector,
    blender_exit_switch_matrix,
    blender_entry_switch_matrix,
    blender_payload_matrix,
    scan_entry_matrix,
    scan_exit_switch_matrix,
    filter_blend_matrix,
    scan_blend_matrix,
    blender_kernel_coefficients,
    scan_kernel_coefficients,
    scan_switch_blockwise,
    entry_switch_blockwise,
    feature_fade_odds,
    fade_speed_multiplier,
    added_rate_shift,
    initial_hidden_vector,
    filter_exit_matrix,
    scan_exit_matrix,
):
    row_count = sequence_activations.shape[0]
    feature_count = entry_rescale_vector.shape[0]
    pieces = [
        blender_exit_switch_matrix,
        blender_entry_switch_matrix,
        blender_payload_matrix,
        scan_entry_matrix,
        scan_exit_switch_matrix,
        filter_blend_matrix,
        scan_blend_matrix,
    ]
    local_cat = jnp.concatenate(pieces, axis=1)
    whole_weight = lax.all_gather(local_cat, "sp", axis=0, tiled=True)
    piece = lax.all_gather(sequence_activations, "tp", axis=1, tiled=True)
    piece_float = piece.astype(jnp.float32)
    scaled_piece = (piece.astype(jnp.float32) * entry_rescale_vector[None, :]).astype(jnp.bfloat16)
    totals = jnp.dot(scaled_piece, whole_weight, preferred_element_type=jnp.float32)
    squares = jnp.sum(piece_float * piece_float, axis=1)
    inverse = lax.rsqrt(squares / feature_count + norm_eps)
    projected = (totals * inverse[:, None]).astype(jnp.bfloat16)
    outputs = []
    offset = 0
    for weight in pieces:
        outputs.append(projected[:, offset : offset + weight.shape[1]])
        offset = offset + weight.shape[1]
    conv_b, conv_c, conv_x, lru_in, lru_gate, mix_conv, mix_lru = outputs
    short_in = conv_c.astype(jnp.float32) * conv_x.astype(jnp.float32)
    lru_float = lru_in.astype(jnp.float32)
    short_edge = blender_kernel_coefficients.shape[0] - 1
    lru_edge = scan_kernel_coefficients.shape[0] - 1
    prev_short, prev_lru = passed_along(
        (short_in[row_count - short_edge :], lru_float[row_count - lru_edge :]), "sp", 1
    )
    lru_conv = causal_local(prev_lru, lru_float, scan_kernel_coefficients).astype(jnp.bfloat16)
    head_local = scan_switch_blockwise.shape[0]
    head_size = scan_switch_blockwise.shape[1]
    lru_local = lru_conv.shape[1]
    heads = lru_conv.reshape(row_count, head_local, head_size)
    scan_switch_amount = jax.nn.sigmoid(
        jnp.einsum("thi,hij->thj", heads, scan_switch_blockwise, preferred_element_type=jnp.float32)
    ).reshape(row_count, lru_local)
    gate_i = jax.nn.sigmoid(
        jnp.einsum(
            "thi,hij->thj", heads, entry_switch_blockwise, preferred_element_type=jnp.float32
        )
    ).reshape(row_count, lru_local)
    position = lax.axis_index("sp") * row_count + jnp.arange(row_count, dtype=jnp.int32)
    fade_exponent_multiplier = (
        scan_switch_exponent
        * scan_switch_amount
        * jax.nn.log_sigmoid(feature_fade_odds)[None, :]
        * fade_speed_multiplier[:, None]
        + added_rate_shift[:, None]
    )
    decay = jnp.exp(fade_exponent_multiplier)
    scale = jnp.sqrt(-jnp.expm1(2.0 * fade_exponent_multiplier))
    scale = jnp.where((position == 0)[:, None], jnp.float32(1.0), scale)
    drive = scale * gate_i * lru_conv.astype(jnp.float32)
    cum_decay, cum_drive = lax.associative_scan(linear_chain, (decay, drive), axis=0)
    ones_state = jnp.ones((lru_local,), jnp.float32)
    zero_state = jnp.zeros((lru_local,), jnp.float32)
    pref_decay, pref_state = entering(
        (cum_decay[-1], cum_drive[-1]), "sp", linear_chain, (ones_state, zero_state)
    )
    carry_in = pref_decay * initial_hidden_vector + pref_state
    state = cum_drive + cum_decay * carry_in[None, :]
    lru_mix = (state * jax.nn.gelu(lru_gate.astype(jnp.float32), approximate=True)).astype(
        jnp.bfloat16
    )
    conv_mix = (
        conv_b.astype(jnp.float32) * causal_local(prev_short, short_in, blender_kernel_coefficients)
    ).astype(jnp.bfloat16)
    conv_part = jnp.dot(conv_mix, filter_exit_matrix, preferred_element_type=jnp.float32)
    lru_part = jnp.dot(lru_mix, scan_exit_matrix, preferred_element_type=jnp.float32)
    conv_sum, lru_sum = (
        lax.psum_scatter(
            conv_part.astype(jnp.bfloat16), "tp", scatter_dimension=1, tiled=True
        ).astype(jnp.float32),
        lax.psum_scatter(
            lru_part.astype(jnp.bfloat16), "tp", scatter_dimension=1, tiled=True
        ).astype(jnp.float32),
    )
    mixed = (
        jax.nn.sigmoid(mix_conv.astype(jnp.float32)) * conv_sum
        + jax.nn.sigmoid(mix_lru.astype(jnp.float32)) * lru_sum
    )
    return mixed.astype(jnp.bfloat16)


def solution(mesh):
    placed = (
        P("sp", "tp"),
        P(),
        P("sp", "tp"),
        P("sp", "tp"),
        P("sp", "tp"),
        P("sp", "tp"),
        P("sp", "tp"),
        P("sp", "tp"),
        P("sp", "tp"),
        P(None, "tp"),
        P(None, "tp"),
        P("tp", None, None),
        P("tp", None, None),
        P("tp"),
        P("sp"),
        P("sp"),
        P("tp"),
        P("tp", None),
        P("tp", None),
    )
    return jax.shard_map(
        local, mesh=mesh, in_specs=placed, out_specs=P("sp", "tp"), check_vma=False
    )
```

profile of v0, /device:TPU:0, one launch (start us, length us, event | category | flops | bytes accessed | tf_op | source)
XLA Modules:
  0.0 475.5 jit_solution(15577859545988110399)
XLA Ops:
  7.3 1.7 constant_dynamic-update-slice_fusion.6
  9.0 1.7 constant_dynamic-update-slice_fusion.5
  10.7 1.7 constant_dynamic-update-slice_fusion.4
  15.7 18.6 %all-gather.5.cloned.1.call-done = bf16[512,2048]{1,0:T(8,128)(2,1)} async-done(((bf16[512,512]{1,0:T(8,128)(2,1)}), bf16[512,2048]{1,0:T(8,128)(2,1)}) %all-gather.5.cloned.1.call-update) | async-done | bytes 2097168 | tf_op jit(solution)/shard_map/all_gather | solution.py:83
  34.2 2.1 fusion.1
  36.3 201.8 %all-gather.7.cloned.1.call-done = bf16[2048,3584]{1,0:T(8,128)(2,1)} async-done(((bf16[256,3584]{1,0:T(8,128)(2,1)}), bf16[2048,3584]{1,0:T(8,128)(2,1)}) %all-gather.7.cloned.1.call-update) | async-done | bytes 14680080 | tf_op jit(solution)/shard_map/all_gather | solution.py:82
  238.1 11.6 %multiply_convert_fusion = bf16[512,3584]{1,0:T(8,128)(2,1)S(1)} fusion(bf16[2048,3584]{1,0:T(8,128)(2,1)} %all-gather.7.cloned.1.call-done, f32[512]{0:T(512)S(1)} %add_rsqrt_fusion, bf16[512,2048]{1,0:T(8,128)(2,1)} %all-gather.5.cloned.1.call-done, f32[2048]{0:T(1024)S(1)} %copy-done.51), kind=kOutput, calls=%fused_computation.4 | convolution fusion | flops 7523008512 | bytes 20457472 | tf_op jit(solution)/shard_map/dot_general | solution.py:86
  250.0 2.5 collective-permute-start
  252.6 2.5 collective-permute-start.1
  255.1 2.8 convolution_convert_fusion.1
  260.8 1.3 copy.35
  262.1 2.6 convert_multiply_fusion.5
  264.7 2.1 slice.352
  266.8 2.1 slice.353
  268.9 2.1 slice.351
  271.0 2.1 slice.355
  273.0 2.0 multiply_add_fusion.1
  275.0 1.4 slice.358
  276.4 1.4 slice.359
  277.8 1.4 slice.357
  279.1 1.4 slice.361
  280.5 2.0 multiply_add_fusion.2
  283.9 1.6 slice.363
  285.5 1.6 slice.367
  287.1 1.8 multiply_add_fusion.3
  290.2 1.5 slice.369
  291.7 1.5 slice.373
  293.2 1.6 multiply_add_fusion.4
  294.9 1.5 slice.376
  296.3 1.4 slice.377
  297.8 1.5 slice.375
  299.2 1.5 slice.379
  300.7 1.4 multiply_add_fusion.5
  302.1 1.4 slice.382
  303.5 1.4 slice.383
  304.8 1.4 slice.381
  306.2 1.4 slice.385
  307.5 1.4 multiply_add_fusion.6
  310.1 1.3 slice.387
  311.4 1.3 slice.391
  312.8 1.4 multiply_add_fusion.7
  320.1 1.4 fusion.68
  322.1 1.3 slice.386
  326.7 1.4 slice.405
  330.6 1.5 slice.374
  332.1 1.5 slice.407
  336.2 1.5 slice.368
  344.1 1.4 slice.356
  345.5 1.4 slice.413
  348.1 2.1 slice.350
  350.2 2.1 slice.415
  354.7 1.9 fusion.51
  357.8 1.7 pad_maximum_fusion.5
  359.5 2.6 pad.142
  362.1 1.7 pad.143
  363.8 2.9 fusion.39
  367.7 4.6 pad.127
  373.3 26.1 %all-gather.1 = f32[8,1,512]{2,1,0:T(1,128)S(1)} all-gather(f32[1,1,512]{2,1,0:T(1,128)S(1)} %add_bitcast_fusion), channel_id=1, replica_groups=mesh['sp'=8,'tp'=4] {'sp'}, dimensions={0}, use_global_device_ids=true | all-gather | bytes 18432 | tf_op jit(solution)/shard_map/all_gather | solution.py:18
  399.5 2.7 pad.145
  402.3 2.7 pad.144
  405.7 26.1 %all-gather = f32[8,1,512]{2,1,0:T(1,128)S(1)} all-gather(f32[1,1,512]{2,1,0:T(1,128)S(1)} %add_bitcast_fusion.1), channel_id=1, replica_groups=mesh['sp'=8,'tp'=4] {'sp'}, dimensions={0}, use_global_device_ids=true | all-gather | bytes 18432 | tf_op jit(solution)/shard_map/all_gather | solution.py:18
  432.3 5.3 %convolution_convert_fusion = bf16[512,2048]{1,0:T(8,128)(2,1)} fusion(bf16[512,2048]{1,0:T(8,128)(2,1)} %param.39, f32[512,512]{1,0:T(8,128)} %pad.144, f32[512,512]{1,0:T(8,128)} %pad.145, f32[512,512]{1,0:T(8,128)S(1)} %copy-done.10, f32[512,512]{1,0:T(8,128)S(1)} %copy-done.8, bf16[512,3584]{1,0:T(8,128)(2,1)} %copy-done.7, f32[512]{0:T(512)S(1)} %multiply_add_fusion.9), kind=kOutput, calls=%fused_computation.9 | convolution fusion | flops 1078722560 | bytes 8914944 | tf_op jit(solution)/shard_map/dot_general | solution.py:143
  437.7 28.3 %reduce-scatter.5.cloned.1.call-done = bf16[512,512]{1,0:T(8,128)(2,1)} async-done(((bf16[512,2048]{1,0:T(8,128)(2,1)}), bf16[512,512]{1,0:T(8,128)(2,1)}) %reduce-scatter.5.cloned.1.call-update) | async-done | bytes 524304 | tf_op jit(solution)/shard_map/reduce_scatter | solution.py:148
  466.1 2.9 add_convert_fusion
  (248 shorter events, 39.9 us)
Async XLA Ops:
  6.5 248.5 %copy-start = (bf16[512,2048]{1,0:T(8,128)(2,1)S(1)}, bf16[512,2048]{1,0:T(8,128)(2,1)}, u32[]{:S(2)}) copy-start(bf16[512,2048]{1,0:T(8,128)(2,1)} %param.38) | copy-start | bytes 6291460
  6.5 5.9 %copy-start.12 = (bf16[256,512]{1,0:T(8,128)(2,1)S(1)}, bf16[256,512]{1,0:T(8,128)(2,1)}, u32[]{:S(2)}) copy-start(bf16[256,512]{1,0:T(8,128)(2,1)} %param.26) | copy-start | bytes 786436
  6.5 6.6 %copy-start.13 = (bf16[256,512]{1,0:T(8,128)(2,1)S(1)}, bf16[256,512]{1,0:T(8,128)(2,1)}, u32[]{:S(2)}) copy-start(bf16[256,512]{1,0:T(8,128)(2,1)} %param.27) | copy-start | bytes 786436
  6.5 7.4 %copy-start.14 = (bf16[256,512]{1,0:T(8,128)(2,1)S(1)}, bf16[256,512]{1,0:T(8,128)(2,1)}, u32[]{:S(2)}) copy-start(bf16[256,512]{1,0:T(8,128)(2,1)} %param.28) | copy-start | bytes 786436
  6.5 8.1 %copy-start.15 = (bf16[256,512]{1,0:T(8,128)(2,1)S(1)}, bf16[256,512]{1,0:T(8,128)(2,1)}, u32[]{:S(2)}) copy-start(bf16[256,512]{1,0:T(8,128)(2,1)} %param.29) | copy-start | bytes 786436
  6.5 27.7 %all-gather.5.cloned.1.call-start = ((), (), s32[]{:S(2)}) async-start(), calls=%async_computation.2 | async-start | bytes 2621440 | tf_op jit(solution)/shard_map/all_gather | solution.py:83
  7.3 230.9 %all-gather.7.cloned.1.call-start = ((), (), s32[]{:S(2)}) async-start(), calls=%async_computation.3 | async-start | bytes 16515072 | tf_op jit(solution)/shard_map/all_gather | solution.py:82
  12.4 3.2 copy-start.47
  12.4 3.2 copy-start.28
  12.4 3.2 copy-start.25
  15.5 222.7 %copy-start.51 = (f32[2048]{0:T(1024)S(1)}, f32[2048]{0:T(1024)}, u32[]{:S(2)}) copy-start(f32[2048]{0:T(1024)} %param.22) | copy-start | bytes 24580
  15.5 422.3 %reduce-scatter.3.cloned.1.call-start = ((), (), s32[]{:S(2)}) async-start(), calls=%async_computation.4 | async-start | bytes 2621440 | tf_op jit(solution)/shard_map/reduce_scatter | solution.py:145
  249.8 5.3 %copy-start.7 = (bf16[512,3584]{1,0:T(8,128)(2,1)}, bf16[512,3584]{1,0:T(8,128)(2,1)S(1)}, u32[]{:S(2)}) copy-start(bf16[512,3584]{1,0:T(8,128)(2,1)S(1)} %multiply_convert_fusion) | copy-start | bytes 11010052
  250.0 5.1 %collective-permute-start = (f32[2,512]{1,0:T(2,128)S(1)}, f32[2,512]{1,0:T(2,128)S(1)}, u32[]{:S(2)}, u32[]{:S(2)}) collective-permute-start(f32[2,512]{1,0:T(2,128)S(1)} %slice.440), channel_id=1, source_target_pairs={{0,4},{4,8},{8,12},{12,16},{16,20},{20,24},{24,28},{1,5},{5,9},{9,... | collective-permute-start | bytes 12296 | tf_op jit(solution)/shard_map/ppermute | solution.py:13
  252.6 5.5 %collective-permute-start.1 = (f32[3,512]{1,0:T(4,128)S(1)}, f32[3,512]{1,0:T(4,128)S(1)}, u32[]{:S(2)}, u32[]{:S(2)}) collective-permute-start(f32[3,512]{1,0:T(4,128)S(1)} %slice.445), channel_id=1, source_target_pairs={{0,4},{4,8},{8,12},{12,16},{16,20},{20,24},{24,28},{1,5},{5,9},{9,... | collective-permute-start | bytes 18440 | tf_op jit(solution)/shard_map/ppermute | solution.py:13
  257.9 0.9 copy-start.49
  257.9 208.2 %reduce-scatter.5.cloned.1.call-start = ((), (), s32[]{:S(2)}) async-start(), calls=%async_computation.5 | async-start | bytes 2621440 | tf_op jit(solution)/shard_map/reduce_scatter | solution.py:148
  258.6 1.1 copy-start.4
  259.3 1.0 copy-start.50
  260.7 1.3 copy-start.45
  260.8 1.3 copy-start.46
  343.9 8.4 %copy-start.41 = (f32[1,512]{1,0:T(1,128)S(1)}, f32[1,512]{1,0:T(1,128)}, u32[]{:S(2)}) copy-start(f32[1,512]{1,0:T(1,128)} %get-tuple-element.182) | copy-start | bytes 6148
  343.9 8.4 %copy-start.42 = (f32[1,512]{1,0:T(1,128)S(1)}, f32[1,512]{1,0:T(1,128)}, u32[]{:S(2)}) copy-start(f32[1,512]{1,0:T(1,128)} %get-tuple-element.183) | copy-start | bytes 6148
  343.9 8.4 %copy-start.43 = (f32[1,512]{1,0:T(1,128)S(1)}, f32[1,512]{1,0:T(1,128)}, u32[]{:S(2)}) copy-start(f32[1,512]{1,0:T(1,128)} %get-tuple-element.184) | copy-start | bytes 6148
  343.9 8.4 %copy-start.44 = (f32[1,512]{1,0:T(1,128)S(1)}, f32[1,512]{1,0:T(1,128)}, u32[]{:S(2)}) copy-start(f32[1,512]{1,0:T(1,128)} %get-tuple-element.185) | copy-start | bytes 6148
  343.9 8.4 %copy-start.27 = (f32[2,512]{1,0:T(2,128)S(1)}, f32[2,512]{1,0:T(2,128)}, u32[]{:S(2)}) copy-start(f32[2,512]{1,0:T(2,128)} %get-tuple-element.202) | copy-start | bytes 12292
  344.0 8.4 %copy-start.26 = (f32[2,512]{1,0:T(2,128)S(1)}, f32[2,512]{1,0:T(2,128)}, u32[]{:S(2)}) copy-start(f32[2,512]{1,0:T(2,128)} %get-tuple-element.201) | copy-start | bytes 12292
  344.0 8.5 %copy-start.23 = (f32[3,512]{1,0:T(4,128)S(1)}, f32[3,512]{1,0:T(4,128)}, u32[]{:S(2)}) copy-start(f32[3,512]{1,0:T(4,128)} %slice.386) | copy-start | bytes 18436
  344.0 8.5 %copy-start.24 = (f32[3,512]{1,0:T(4,128)S(1)}, f32[3,512]{1,0:T(4,128)}, u32[]{:S(2)}) copy-start(f32[3,512]{1,0:T(4,128)} %slice.403) | copy-start | bytes 18436
  344.0 8.5 %copy-start.40 = (f32[1,512]{1,0:T(1,128)S(1)}, f32[1,512]{1,0:T(1,128)}, u32[]{:S(2)}) copy-start(f32[1,512]{1,0:T(1,128)} %slice.485) | copy-start | bytes 6148
  344.0 8.6 %copy-start.39 = (f32[1,512]{1,0:T(1,128)S(1)}, f32[1,512]{1,0:T(1,128)}, u32[]{:S(2)}) copy-start(f32[1,512]{1,0:T(1,128)} %slice.456) | copy-start | bytes 6148
  344.0 8.6 %copy-start.22 = (f32[7,512]{1,0:T(8,128)S(1)}, f32[7,512]{1,0:T(8,128)}, u32[]{:S(2)}) copy-start(f32[7,512]{1,0:T(8,128)} %slice.405) | copy-start | bytes 43012
  344.0 8.7 %copy-start.38 = (f32[1,512]{1,0:T(1,128)S(1)}, f32[1,512]{1,0:T(1,128)}, u32[]{:S(2)}) copy-start(f32[1,512]{1,0:T(1,128)} %slice.484) | copy-start | bytes 6148
  344.0 8.7 %copy-start.37 = (f32[1,512]{1,0:T(1,128)S(1)}, f32[1,512]{1,0:T(1,128)}, u32[]{:S(2)}) copy-start(f32[1,512]{1,0:T(1,128)} %slice.455) | copy-start | bytes 6148
  344.0 8.8 %copy-start.18 = (f32[15,512]{1,0:T(8,128)S(1)}, f32[15,512]{1,0:T(8,128)}, u32[]{:S(2)}) copy-start(f32[15,512]{1,0:T(8,128)} %slice.374) | copy-start | bytes 92164
  344.0 8.8 %copy-start.19 = (f32[15,512]{1,0:T(8,128)S(1)}, f32[15,512]{1,0:T(8,128)}, u32[]{:S(2)}) copy-start(f32[15,512]{1,0:T(8,128)} %slice.407) | copy-start | bytes 92164
  344.1 8.8 %copy-start.36 = (f32[1,512]{1,0:T(1,128)S(1)}, f32[1,512]{1,0:T(1,128)}, u32[]{:S(2)}) copy-start(f32[1,512]{1,0:T(1,128)} %slice.483) | copy-start | bytes 6148
  345.5 7.5 %copy-start.35 = (f32[1,512]{1,0:T(1,128)S(1)}, f32[1,512]{1,0:T(1,128)}, u32[]{:S(2)}) copy-start(f32[1,512]{1,0:T(1,128)} %slice.454) | copy-start | bytes 6148
  348.1 5.0 %copy-start.16 = (f32[31,512]{1,0:T(8,128)S(1)}, f32[31,512]{1,0:T(8,128)}, u32[]{:S(2)}) copy-start(f32[31,512]{1,0:T(8,128)} %slice.368) | copy-start | bytes 190468
  348.1 5.0 %copy-start.17 = (f32[31,512]{1,0:T(8,128)S(1)}, f32[31,512]{1,0:T(8,128)}, u32[]{:S(2)}) copy-start(f32[31,512]{1,0:T(8,128)} %slice.409) | copy-start | bytes 190468
  350.2 2.9 copy-start.34
  350.2 3.0 copy-start.33
  352.6 0.9 copy-start.11
  352.9 0.7 copy-start.32
  353.1 0.7 copy-start.31
  353.8 2.8 copy-start.30
  354.7 3.1 copy-start.29
  363.7 3.9 copy-start.2
  363.7 3.9 copy-start.3
  367.6 4.7 copy-start.6
  372.4 29.8 %copy-start.5 = (f32[255,512]{1,0:T(8,128)S(1)}, f32[255,512]{1,0:T(8,128)}, u32[]{:S(2)}) copy-start(f32[255,512]{1,0:T(8,128)} %get-tuple-element.157) | copy-start | bytes 1566724
  372.6 26.9 %copy-start.9 = (f32[512,512]{1,0:T(8,128)}, f32[512,512]{1,0:T(8,128)S(1)}, u32[]{:S(2)}) copy-start(f32[512,512]{1,0:T(8,128)S(1)} %pad.126) | copy-start | bytes 3145732
  399.4 32.4 %copy-start.20 = (f32[512]{0:T(512)S(1)}, f32[512]{0:T(512)}, u32[]{:S(2)}) copy-start(f32[512]{0:T(512)} %custom-call) | copy-start | bytes 6148
  399.4 32.4 %copy-start.21 = (f32[512]{0:T(512)S(1)}, f32[512]{0:T(512)}, u32[]{:S(2)}) copy-start(f32[512]{0:T(512)} %custom-call.1) | copy-start | bytes 6148
  399.5 32.9 %copy-start.48 = (f32[512]{0:T(512)S(1)}, f32[512]{0:T(512)}, u32[]{:S(2)}) copy-start(f32[512]{0:T(512)} %param.37) | copy-start | bytes 6148
  399.5 32.9 %copy-start.8 = (f32[512,512]{1,0:T(8,128)S(1)}, f32[512,512]{1,0:T(8,128)}, u32[]{:S(2)}) copy-start(f32[512,512]{1,0:T(8,128)} %pad.127) | copy-start | bytes 3145732
  402.2 30.1 %copy-start.10 = (f32[512,512]{1,0:T(8,128)S(1)}, f32[512,512]{1,0:T(8,128)}, u32[]{:S(2)}) copy-start(f32[512,512]{1,0:T(8,128)} %copy-done.9) | copy-start | bytes 3145732
  437.7 31.3 %copy-start.1 = (bf16[512,2048]{1,0:T(8,128)(2,1)S(1)}, bf16[512,2048]{1,0:T(8,128)(2,1)}, u32[]{:S(2)}) copy-start(bf16[512,2048]{1,0:T(8,128)(2,1)} %param.38) | copy-start | bytes 6291460
Sparse Core Ops, SparseCore 0:
  8.9 25.2 all-gather.4
  36.4 201.6 all-gather.6
  258.0 30.6 reduce-scatter.2
  437.8 28.1 reduce-scatter.4
where the time goes:
time: 478 us; the launch traced here: 476 us
  waiting for transfers between devices  249 us (52%)
  local copies, waits for them, and re-layouts  100 us (21%)
  blocking collectives  52.2 us (11%)
  other arithmetic  33 us (7%)
  matrix products  20.7 us (4%)
  between operations  14.2 us (3%)
  starting transfers between devices  5.26 us (1%)
    all_gather x1, waiting for transfers between devices, local(): whole_weight = lax.all_gather(local_cat, 'sp', axis=0, tiled=True)  202 us
    slice x60, local copies, waits for them, and re-layouts, local(): lax.associative_scan(linear_chain, (decay, drive), axis=0)  73.1 us
    all_gather x2, blocking collectives, entering(): everything = jax.tree.map(lambda part: lax.all_gather(part, axis), value)  52.2 us
    reduce_scatter x1, waiting for transfers between devices, local(): lax.psum_scatter(lru_part.astype(jnp.bfloat16), 'tp', scatter_dimension=1...  28.3 us
    all_gather x1, waiting for transfers between devices, local(): piece = lax.all_gather(sequence_activations, 'tp', axis=1, tiled=True)  18.6 us
    add x16, other arithmetic, linear_chain(): return (earlier[0] * later[0], later[0] * earlier[1] + later[1])  17.2 us
    pad x32, local copies, waits for them, and re-layouts, local(): lax.associative_scan(linear_chain, (decay, drive), axis=0)  16 us
    dot_general x1, matrix products, local(): jnp.dot(scaled_piece, whole_weight, preferred_element_type=jnp.float32)  11.6 us
  transfers between devices with their start and end apart: 6, of which 3 were waited for; matrix products, arithmetic and copies ran while one was open for 29% of the time, Pallas kernels for 0%

commit v1 on v0

--- a/solution.py
+++ b/solution.py
@@ -1,6 +1,10 @@
+import functools
+
 import jax
 import jax.numpy as jnp
 from jax import lax
+from jax.experimental import pallas as pl
+from jax.experimental.pallas import tpu as pltpu
 from jax.sharding import PartitionSpec as P
 
 scan_switch_exponent = 8.0
@@ -156,6 +160,558 @@
     return mixed.astype(jnp.bfloat16)
 
 
+MESH = pl.DeviceIdType.MESH
+F32, BF16 = jnp.float32, jnp.bfloat16
+
+
+def small_log1p(u):
+    w = 1.0 + u
+    return jnp.where(w == 1.0, u, jnp.log(w) * u / jnp.where(w == 1.0, 1.0, w - 1.0))
+
+
+def neg_expm1(v):
+    near = 1.0 + v * (1.0 / 8.0)
+    for n in (7, 6, 5, 4, 3, 2):
+        near = 1.0 + v * (1.0 / n) * near
+    return jnp.where(v > -0.5, -v * near, 1.0 - jnp.exp(v))
+
+
+def fused_kernel(
+    sizes,
+    x_hbm, gain, w0, w1, w2, w3, w4, w5, w6,
+    ctaps, ltaps, wr, wi, odds, pos, init, ec_hbm, el_hbm,
+    out,
+    wbuf, xg, xs, sq, inv, posn, lbuf, abuf, bbuf, cbuf, carry_in, carry_out, sbuf,
+    mix, got, parts, rbuf, sums, ebuf,
+    wl, wx_s, wx_r, zr_s, zr_r, zl_s, zl_r, xg_s, xg_r, po_s, po_r, ed_s, ed_r,
+    xe_s, xe_r, rs_s, rs_r, loc,
+):
+    sp, tp = sizes
+    nz = sp // 2
+    s, t = lax.axis_index("sp"), lax.axis_index("tp")
+    z, x = s // 2, lax.rem(s, 2)
+    xo = 1 - x
+    half = wbuf.shape[3]
+    rows = x_hbm.shape[0]
+    krows = w0.shape[0]
+    feats = x_hbm.shape[1]
+    both = 2 * rows
+    tile = half
+    segs = 8
+    seg = both // segs
+    weights = (w0, w1, w2, w3, w4, w5, w6)
+    count = len(weights)
+    xn = (s + 1 - 2 * x, t)
+    core = t + 1 - 2 * lax.rem(t, 2)
+    ty = lax.rem(t + 2, tp)
+    tyc = lax.rem(core + 2, tp)
+    has_l, has_r = z > 0, z < nz - 1
+    left, right = (s - 2, t), (s + 2, t)
+
+    def remote(src, dst, ss, rs, dev):
+        return pltpu.make_async_remote_copy(
+            src_ref=src, dst_ref=dst, send_sem=ss, recv_sem=rs, device_id=dev, device_id_type=MESH
+        )
+
+    bar = pltpu.get_barrier_semaphore()
+    pl.semaphore_signal(bar, inc=1, device_id=xn, device_id_type=MESH)
+    for j in range(1, tp):
+        pl.semaphore_signal(bar, inc=1, device_id=(s, lax.rem(t + j, tp)), device_id_type=MESH)
+
+    @pl.when(has_l)
+    def _():
+        pl.semaphore_signal(bar, inc=1, device_id=left, device_id_type=MESH)
+
+    @pl.when(has_r)
+    def _():
+        pl.semaphore_signal(bar, inc=1, device_id=right, device_id_type=MESH)
+
+    own_cols = pl.ds(pl.multiple_of(x * half, half), half)
+    other_cols = pl.ds(pl.multiple_of(xo * half, half), half)
+
+    def own_half(p):
+        return pltpu.make_async_copy(
+            weights[p].at[:, own_cols], wbuf.at[p, z, x], wl.at[p]
+        )
+
+    def swap_half(p):
+        return remote(weights[p].at[:, other_cols], wbuf.at[p, z, x], wx_s.at[p], wx_r.at[p], xn)
+
+    def swap_half_in(p):
+        return remote(weights[p].at[:, other_cols], wbuf.at[p, z, xo], wx_s.at[p], wx_r.at[p], xn)
+
+    x_in = pltpu.make_async_copy(x_hbm, xg.at[x, t], loc.at[2])
+    exits = (
+        pltpu.make_async_copy(el_hbm, ebuf.at[0], loc.at[0]),
+        pltpu.make_async_copy(ec_hbm, ebuf.at[1], loc.at[1]),
+    )
+    x_in.start()
+    for p in range(count):
+        own_half(p).start()
+    pl.semaphore_wait(bar, tp + jnp.where(has_l, 1, 0) + jnp.where(has_r, 1, 0))
+
+    swap_half(0).start()
+    x_moves = {
+        0: lambda: remote(x_hbm, xg.at[x, t], xg_s.at[0], xg_r.at[0], xn),
+        1: lambda: remote(x_hbm, xg.at[x, t], xg_s.at[1], xg_r.at[1], (s, ty)),
+        2: lambda: remote(x_hbm, xg.at[x, t], xg_s.at[2], xg_r.at[2], (s, core)),
+        3: lambda: remote(xg.at[xo, t], xg.at[xo, t], xg_s.at[3], xg_r.at[3], (s, ty)),
+        4: lambda: remote(xg.at[xo, t], xg.at[xo, t], xg_s.at[4], xg_r.at[4], (s, core)),
+        5: lambda: remote(xg.at[x, ty], xg.at[x, ty], xg_s.at[5], xg_r.at[5], (s, core)),
+        6: lambda: remote(xg.at[xo, ty], xg.at[xo, ty], xg_s.at[6], xg_r.at[6], (s, core)),
+    }
+    x_slots = {
+        0: (xo, t), 1: (x, ty), 2: (x, core), 3: (xo, ty),
+        4: (xo, core), 5: (x, tyc), 6: (xo, tyc),
+    }
+
+    def x_arrive(k):
+        a, b = x_slots[k]
+        remote(xg.at[a, b], xg.at[a, b], xg_s.at[k], xg_r.at[k], (s, core)).wait_recv()
+
+    for k in (0, 1, 2):
+        x_moves[k]().start()
+    pos_out = remote(pos, posn.at[x], po_s, po_r, xn)
+    pos_out.start()
+    for p in range(1, count):
+        swap_half(p).start()
+    for e in exits:
+        e.start()
+
+    def z_right(p, d):
+        ref = wbuf.at[p, z - d]
+        return remote(ref, ref, zr_s.at[p, d], zr_r.at[p, d], right)
+
+    def z_left(p, d):
+        ref = wbuf.at[p, z + d]
+        return remote(ref, ref, zl_s.at[p, d], zl_r.at[p, d], left)
+
+    def from_left(p, d):
+        ref = wbuf.at[p, z - 1 - d]
+        return remote(ref, ref, zr_s.at[p, d], zr_r.at[p, d], right)
+
+    def from_right(p, d):
+        ref = wbuf.at[p, z + 1 + d]
+        return remote(ref, ref, zl_s.at[p, d], zl_r.at[p, d], left)
+
+    def issue_own(p):
+        if p >= count:
+            return
+        own_half(p).wait()
+        swap_half_in(p).wait_recv()
+
+        @pl.when(has_r)
+        def _():
+            z_right(p, 0).start()
+
+        @pl.when(has_l)
+        def _():
+            z_left(p, 0).start()
+
+    relayed = set()
+
+    def relay(p, d):
+        if p >= count or d >= nz - 1 or (p, d) in relayed:
+            return
+        relayed.add((p, d))
+
+        @pl.when(z - 1 - d >= 0)
+        def _():
+            from_left(p, d).wait_recv()
+            if d + 1 < nz - 1:
+                @pl.when(has_r)
+                def _():
+                    z_right(p, d + 1).start()
+
+        @pl.when(z + 1 + d < nz)
+        def _():
+            from_right(p, d).wait_recv()
+            if d + 1 < nz - 1:
+                @pl.when(has_l)
+                def _():
+                    z_left(p, d + 1).start()
+
+    def scale_block(a, b):
+        for i in range(rows // tile):
+            piece = xg[a, b, pl.ds(i * tile, tile), :].astype(F32)
+            at = pl.ds(pl.multiple_of(a * rows + i * tile, tile), tile)
+            xs[b, at, :] = (piece * gain[b]).astype(BF16)
+            square = piece * piece
+            total = square[:, 0:128]
+            for c in range(1, feats // 128):
+                total = total + square[:, c * 128 : (c + 1) * 128]
+            sq[at, :] += total
+
+    issue_own(0)
+    issue_own(1)
+    sq[...] = jnp.zeros_like(sq)
+    x_in.wait()
+    scale_block(x, t)
+    relay(0, 0)
+    issue_own(2)
+    x_arrive(2)
+    scale_block(x, core)
+    x_arrive(0)
+    x_moves[3]().start()
+    x_moves[4]().start()
+    x_arrive(1)
+    x_moves[5]().start()
+    relay(0, 1)
+    scale_block(xo, t)
+    scale_block(x, ty)
+    x_arrive(3)
+    x_moves[6]().start()
+    relay(0, 2)
+    scale_block(xo, ty)
+    x_arrive(4)
+    scale_block(xo, core)
+    x_arrive(5)
+    scale_block(x, tyc)
+    relay(1, 0)
+    x_arrive(6)
+    scale_block(xo, tyc)
+    total = jnp.sum(sq[...], axis=1, keepdims=True)
+    inv[...] = jnp.broadcast_to(lax.rsqrt(total / (feats * tp) + norm_eps), inv.shape)
+    posn[x] = pos[...]
+    remote(pos, posn.at[xo], po_s, po_r, xn).wait_recv()
+
+    def project(p, use):
+        per = krows * 2
+
+        def step(i, _):
+            at = pl.ds(pl.multiple_of(i * tile, tile), tile)
+            acc = None
+            for b in range(tp):
+                lhs = xs[b, at, :]
+                for zz in range(b * feats // per, (b + 1) * feats // per):
+                    for xx in range(2):
+                        k0 = zz * per + xx * krows - b * feats
+                        term = jnp.dot(
+                            lhs[:, k0 : k0 + krows], wbuf[p, zz, xx], preferred_element_type=F32
+                        )
+                        acc = term if acc is None else acc + term
+            wide = inv[at, :]
+            scale = jnp.concatenate([wide] * (half // 128), axis=1)
+            use(at, i, (acc * scale).astype(BF16))
+            return 0
+
+        lax.fori_loop(0, both // tile, step, 0)
+
+    def edge(buf, k):
+        return remote(buf.at[pl.ds(both, 8)], buf.at[pl.ds(0, 8)], ed_s.at[k], ed_r.at[k], right)
+
+    def edge_send(buf, k):
+        @pl.when(has_r)
+        def _():
+            edge(buf, k).start()
+
+        @pl.when(z == 0)
+        def _():
+            buf[0:8, :] = jnp.zeros((8, half), F32)
+
+    def edge_wait(buf, k):
+        @pl.when(has_l)
+        def _():
+            edge(buf, k).wait_recv()
+
+    def carry_copy():
+        return remote(carry_out, carry_in, ed_s.at[2], ed_r.at[2], right)
+
+    def swap(k):
+        at = pl.ds(pl.multiple_of(xo * rows, rows), rows)
+        return remote(mix.at[k, at], got.at[k, x], xe_s.at[k], xe_r.at[k], xn)
+
+    def swap_start(k):
+        swap(k).start()
+        at = pl.ds(pl.multiple_of(x * rows, rows), rows)
+        got[k, x] = mix[k, at, :]
+
+    def swap_wait(k):
+        remote(mix.at[k, pl.ds(0, rows)], got.at[k, xo], xe_s.at[k], xe_r.at[k], xn).wait_recv()
+
+    def exchange(e, j):
+        peer = lax.rem(t + j, tp)
+        return remote(parts.at[e, j], rbuf.at[e, j], rs_s.at[e, j], rs_r.at[e, j], (s, peer))
+
+    def exit_matmul(e):
+        exits[e].wait()
+        for j in list(range(1, tp)) + [0]:
+            peer = lax.rem(t + j, tp)
+            cols = pl.ds(pl.multiple_of(peer * feats, feats), feats)
+
+            def step(i, _):
+                at = pl.ds(pl.multiple_of(i * tile, tile), tile)
+                acc = jnp.dot(
+                    got[e, 0, at, :], ebuf[e, 0:half, cols], preferred_element_type=F32
+                ) + jnp.dot(
+                    got[e, 1, at, :], ebuf[e, half : 2 * half, cols], preferred_element_type=F32
+                )
+                parts[e, j, at, :] = acc.astype(BF16)
+                return 0
+
+            lax.fori_loop(0, rows // tile, step, 0)
+            if j > 0:
+                exchange(e, j).start()
+
+    def exit_sum(e):
+        for j in range(1, tp):
+            exchange(e, j).wait_recv()
+        total = parts[e, 0].astype(F32)
+        for j in range(1, tp):
+            total = total + rbuf[e, j].astype(F32)
+        sums[e] = total
+
+    def finish_stage(p):
+        for d in range(nz - 1):
+            relay(p, d)
+        issue_own(p + 3)
+
+    issue_own(3)
+
+    def keep_lru(at, i, value):
+        lbuf[pl.ds(pl.multiple_of(8 + i * tile, 8), tile), :] = value.astype(F32)
+
+    project(0, keep_lru)
+    edge_send(lbuf, 0)
+    relay(1, 1)
+    edge_wait(lbuf, 0)
+    rate = -scan_switch_exponent * small_log1p(jnp.exp(-odds[:, own_cols]))
+    lanes = ltaps[:, own_cols].astype(F32)
+    taps = ltaps.shape[0]
+    for i in range(both // tile):
+        conv = None
+        for k in range(taps):
+            term = lbuf[pl.ds(8 - (taps - 1) + k + i * tile, tile), :] * lanes[k : k + 1]
+            conv = term if conv is None else conv + term
+        conv = conv.astype(BF16)
+        gate_r = jax.nn.sigmoid(jnp.dot(conv, wr[x], preferred_element_type=F32))
+        gate_i = jax.nn.sigmoid(jnp.dot(conv, wi[x], preferred_element_type=F32))
+        first = (i * tile) // rows
+        local_at = i * tile - first * rows
+        turned = posn[first].T
+        speed = turned[local_at : local_at + tile, 0:1]
+        shift = turned[local_at : local_at + tile, 1:2]
+        log_a = gate_r * rate * speed + shift
+        gain_in = jnp.sqrt(neg_expm1(2.0 * log_a))
+        if i == 0:
+            row = lax.broadcasted_iota(jnp.int32, gain_in.shape, 0) + z * both
+            gain_in = jnp.where(row == 0, 1.0, gain_in)
+        decay = jnp.exp(log_a)
+        drive = gain_in * gate_i * conv.astype(F32)
+        for c in range(half // 128):
+            cols = slice(c * 128, (c + 1) * 128)
+            abuf[c, pl.ds(i * tile, tile), :] = decay[:, cols]
+            bbuf[c, pl.ds(i * tile, tile), :] = drive[:, cols]
+
+    lanes_n = half // 128
+
+    def scan_step(i, held):
+        cum, state = list(held[:lanes_n]), list(held[lanes_n:])
+        at = pl.ds(i, segs, stride=seg)
+        for c in range(lanes_n):
+            a = abuf[c, at, :]
+            state[c] = a * state[c] + bbuf[c, at, :]
+            cum[c] = cum[c] * a
+            abuf[c, at, :] = cum[c]
+            bbuf[c, at, :] = state[c]
+        return tuple(cum) + tuple(state)
+
+    ends = lax.fori_loop(
+        0, seg, scan_step,
+        tuple(jnp.ones((segs, 128), F32) for _ in range(lanes_n))
+        + tuple(jnp.zeros((segs, 128), F32) for _ in range(lanes_n)),
+        unroll=8,
+    )
+    end_a = jnp.concatenate(ends[:lanes_n], axis=1)
+    end_b = jnp.concatenate(ends[lanes_n:], axis=1)
+
+    @pl.when(z == 0)
+    def _():
+        carry_in[...] = jnp.broadcast_to(init[:, own_cols], carry_in.shape)
+
+    finish_stage(1)
+
+    @pl.when(has_l)
+    def _():
+        carry_copy().wait_recv()
+
+    carry = carry_in[0:1, :]
+    for j in range(segs):
+        cbuf[j : j + 1, :] = carry
+        carry = end_b[j : j + 1] + end_a[j : j + 1] * carry
+    carry_out[...] = jnp.broadcast_to(carry, carry_out.shape)
+
+    @pl.when(has_r)
+    def _():
+        carry_copy().start()
+
+    def keep_gate(at, i, value):
+        gate = jax.nn.gelu(value.astype(F32), approximate=True)
+        pieces = []
+        for j in range(tile // seg):
+            here = pl.ds(pl.multiple_of(i * tile + j * seg, seg), seg)
+            c = cbuf[pl.ds(i * (tile // seg) + j, 1), :]
+            pieces.append(
+                jnp.concatenate(
+                    [
+                        bbuf[n, here, :] + abuf[n, here, :] * c[:, n * 128 : (n + 1) * 128]
+                        for n in range(half // 128)
+                    ],
+                    axis=1,
+                )
+            )
+        mix[0, at, :] = (jnp.concatenate(pieces, axis=0) * gate).astype(BF16)
+
+    project(1, keep_gate)
+    swap_start(0)
+    finish_stage(2)
+
+    def keep_c(at, i, value):
+        sbuf[pl.ds(pl.multiple_of(8 + i * tile, 8), tile), :] = value.astype(F32)
+
+    project(2, keep_c)
+    swap_wait(0)
+    exit_matmul(0)
+    finish_stage(3)
+
+    def keep_cx(at, i, value):
+        here = pl.ds(pl.multiple_of(8 + i * tile, 8), tile)
+        sbuf[here, :] = sbuf[here, :] * value.astype(F32)
+
+    project(3, keep_cx)
+    edge_send(sbuf, 1)
+    finish_stage(4)
+
+    def keep_b(at, i, value):
+        lbuf[pl.ds(pl.multiple_of(8 + i * tile, 8), tile), :] = value.astype(F32)
+
+    @pl.when(has_r)
+    def _():
+        edge(lbuf, 0).wait_send()
+
+    project(4, keep_b)
+    edge_wait(sbuf, 1)
+    clanes = ctaps[:, own_cols].astype(F32)
+    ktaps = ctaps.shape[0]
+    for i in range(both // tile):
+        conv = None
+        for k in range(ktaps):
+            term = sbuf[pl.ds(8 - (ktaps - 1) + k + i * tile, tile), :] * clanes[k : k + 1]
+            conv = term if conv is None else conv + term
+        mix[1, pl.ds(i * tile, tile), :] = (lbuf[pl.ds(8 + i * tile, tile), :] * conv).astype(BF16)
+    swap_start(1)
+    relay(5, 0)
+    relay(5, 1)
+    swap_wait(1)
+    exit_matmul(1)
+    for d in range(2, nz - 1):
+        relay(5, d)
+
+    def keep_mix(k):
+        def use(at, i, value):
+            mix[k, at, :] = value
+        return use
+
+    project(5, keep_mix(2))
+    swap_start(2)
+    exit_sum(0)
+    for d in range(nz - 1):
+        relay(6, d)
+    project(6, keep_mix(3))
+    swap_start(3)
+    exit_sum(1)
+    swap_wait(2)
+    swap_wait(3)
+    for xx in range(2):
+        cols = slice(xx * half, (xx + 1) * half)
+        out[:, cols] = (
+            jax.nn.sigmoid(got[2, xx].astype(F32)) * sums[1, :, cols]
+            + jax.nn.sigmoid(got[3, xx].astype(F32)) * sums[0, :, cols]
+        ).astype(BF16)
+
+    pos_out.wait_send()
+    for p in range(count):
+        swap_half(p).wait_send()
+        for d in range(nz - 1):
+            @pl.when(has_r & (z - d >= 0))
+            def _():
+                z_right(p, d).wait_send()
+
+            @pl.when(has_l & (z + d < nz))
+            def _():
+                z_left(p, d).wait_send()
+    for k in x_moves:
+        x_moves[k]().wait_send()
+
+    @pl.when(has_r)
+    def _():
+        edge(sbuf, 1).wait_send()
+        carry_copy().wait_send()
+
+    for k in range(4):
+        swap(k).wait_send()
+    for e in range(2):
+        for j in range(1, tp):
+            exchange(e, j).wait_send()
+
+
+def paired(sizes, *args):
+    (
+        x, gain, wb, wc, wx, win, wgate, mconv, mlru, ctaps, ltaps, wr, wi,
+        odds, speed, shift, init, ec, el,
+    ) = args
+    sp, tp = sizes
+    nz = sp // 2
+    rows, feats = x.shape
+    krows, width = wb.shape
+    half = width // 2
+    both = 2 * rows
+    pos = jnp.concatenate(
+        [speed[None], shift[None], jnp.zeros((6, rows), F32)], axis=0
+    )
+    vmem = pl.BlockSpec(memory_space=pltpu.VMEM)
+    anys = pl.BlockSpec(memory_space=pl.ANY)
+    dma = pltpu.SemaphoreType.DMA
+    kernel = pl.pallas_call(
+        functools.partial(fused_kernel, sizes),
+        out_shape=jax.ShapeDtypeStruct((rows, width), BF16),
+        in_specs=[anys, vmem] + [anys] * 7 + [vmem] * 7 + [anys] * 2,
+        out_specs=vmem,
+        scratch_shapes=[
+            pltpu.VMEM((7, nz, 2, krows, half), BF16),
+            pltpu.VMEM((2, tp, rows, feats), BF16),
+            pltpu.VMEM((tp, both, feats), BF16),
+            pltpu.VMEM((both, 128), F32),
+            pltpu.VMEM((both, 128), F32),
+            pltpu.VMEM((2, 8, rows), F32),
+            pltpu.VMEM((both + 8, half), F32),
+            pltpu.VMEM((half // 128, both, 128), F32),
+            pltpu.VMEM((half // 128, both, 128), F32),
+            pltpu.VMEM((8, half), F32),
+            pltpu.VMEM((8, half), F32),
+            pltpu.VMEM((8, half), F32),
+            pltpu.VMEM((both + 8, half), F32),
+            pltpu.VMEM((4, both, half), BF16),
+            pltpu.VMEM((4, 2, rows, half), BF16),
+            pltpu.VMEM((2, tp, rows, feats), BF16),
+            pltpu.VMEM((2, tp, rows, feats), BF16),
+            pltpu.VMEM((2, rows, width), F32),
+            pltpu.VMEM((2,) + ec.shape, BF16),
+            dma((7,)), dma((7,)), dma((7,)),
+            dma((7, nz - 1)), dma((7, nz - 1)), dma((7, nz - 1)), dma((7, nz - 1)),
+            dma((7,)), dma((7,)), dma, dma, dma((3,)), dma((3,)),
+            dma((4,)), dma((4,)), dma((2, tp)), dma((2, tp)), dma((3,)),
+        ],
+        compiler_params=pltpu.CompilerParams(
+            collective_id=0, has_side_effects=True, vmem_limit_bytes=62 * 1024 * 1024
+        ),
+    )
+    return kernel(
+        x, gain.reshape(tp, 1, feats), win, wgate, wc, wx, wb, mconv, mlru,
+        ctaps, ltaps, wr, wi, odds.reshape(1, width), pos, init.reshape(1, width), ec, el,
+    )
+
+
 def solution(mesh):
     placed = (
         P("sp", "tp"),
@@ -178,6 +734,14 @@
         P("tp", None),
         P("tp", None),
     )
+    sizes = (mesh.shape["sp"], mesh.shape["tp"])
+
+    def body(*args):
+        heads = args[11].shape[0]
+        if heads == 2 and sizes[1] == 4 and sizes[0] % 2 == 0 and sizes[0] >= 4:
+            return paired(sizes, *args)
+        return local(*args)
+
     return jax.shard_map(
-        local, mesh=mesh, in_specs=placed, out_specs=P("sp", "tp"), check_vma=False
-    )
+        body, mesh=mesh, in_specs=placed, out_specs=P("sp", "tp"), check_vma=False
+    )

time: 478 us -> 155 us (0.32)
  waiting for transfers between devices: 249 us -> 0 us
  Pallas kernels: 0 us -> 151 us
  local copies, waits for them, and re-layouts: 100 us -> 1.95 us
  blocking collectives: 52.2 us -> 0 us
  other arithmetic: 33 us -> 1.37 us
  matrix products: 20.7 us -> 0 us
  between operations: 14.2 us -> 0.01 us
  starting transfers between devices: 5.26 us -> 0 us
    all_gather x2 -> x0, waiting for transfers between devices: 220 us -> none  [the longest x1 202 us: local(): whole_weight = lax.all_gather(local_cat, 'sp', axis=0, tiled=True)]
    pallas_call x0 -> x1, Pallas kernels: none -> 151 us  [paired(): kernel(x, gain.reshape(tp, 1, feats), win, wgate, wc, wx, wb, mconv, mlru...]
    slice x62 -> x0, local copies, waits for them, and re-layouts: 73.1 us -> none  [the longest x60 73.1 us: local(): lax.associative_scan(linear_chain, (decay, drive), axis=0)]
    all_gather x2 -> x0, blocking collectives: 52.2 us -> none  [entering(): everything = jax.tree.map(lambda part: lax.all_gather(part, axis), value)]
    reduce_scatter x2 -> x0, waiting for transfers between devices: 28.4 us -> none  [the longest x1 28.3 us: local(): lax.psum_scatter(lru_part.astype(jnp.bfloat16), 'tp', scatter_dimension=1...]
    dot_general x5 -> x0, matrix products: 20.7 us -> none  [the longest x1 11.6 us: local(): jnp.dot(scaled_piece, whole_weight, preferred_element_type=jnp.float32)]
    add x32 -> x0, other arithmetic: 19.7 us -> none  [the longest x16 17.2 us: linear_chain(): return (earlier[0] * later[0], later[0] * earlier[1] + later[1])]
    pad x32 -> x0, local copies, waits for them, and re-layouts: 16 us -> none  [local(): lax.associative_scan(linear_chain, (decay, drive), axis=0)]
  transfers between devices with their start and end apart: 6 -> 0, of which waited for: 3 -> 0; matrix products, arithmetic and copies ran while one was open for 29% -> 0% of each run, Pallas kernels for 0% -> 0%
where the time goes in v1:
time: 155 us; the launch traced here: 154 us
  Pallas kernels  151 us (97%)
  local copies, waits for them, and re-layouts  1.95 us (1%)
    pallas_call x1, Pallas kernels, paired(): kernel(x, gain.reshape(tp, 1, feats), win, wgate, wc, wx, wb, mconv, mlru...  151 us

profile of v1, /device:TPU:0, one launch (start us, length us, event | category | flops | bytes accessed | tf_op | source)
XLA Modules:
  0.0 154.3 jit_solution(16007128981074054053)
XLA Ops:
  0.0 0.1 pad.2.clone
  0.1 1.4 maximum_maximum_fusion.pos
  1.5 151.0 %shard_map.181 = bf16[512,512]{1,0:T(8,128)(2,1)} custom-call(bf16[512,512]{1,0:T(8,128)(2,1)} %x_hbm.1, f32[4,1,512]{2,1,0:T(1,128)} %bitcast.5, bf16[256,512]{1,0:T(8,128)(2,1)} %w0.1, bf16[256,512]{1,0:T(8,128)(2,1)} %w1.1, bf16[256,512]{1,0:T(8,128)(2,1)} %w2.1, bf16[256,512]{1,0:T(8,128)(2,1)} %w3.1, bf16[256,512]{1,0:T(8,128)(2,1)} %w4.1, ...), custom_call_target="tpu_custom_call" | custom-call | tf_op jit(solution)/shard_map/pallas_call | solution.py:709
  152.4 1.9 %copy.21 = bf16[512,512]{1,0:T(8,128)(2,1)} copy(bf16[512,512]{1,0:T(8,128)(2,1)} %shard_map.181) | data formatting | bytes 1048576
  (1 shorter events, 0.0 us)

commit v2 on v1

--- a/solution.py
+++ b/solution.py
@@ -184,7 +184,7 @@
     wbuf, xg, xs, sq, inv, posn, lbuf, abuf, bbuf, cbuf, carry_in, carry_out, sbuf,
     mix, got, parts, rbuf, sums, ebuf,
     wl, wx_s, wx_r, zr_s, zr_r, zl_s, zl_r, xg_s, xg_r, po_s, po_r, ed_s, ed_r,
-    xe_s, xe_r, rs_s, rs_r, loc,
+    xe_s, xe_r, rs_s, rs_r, loc, fi_s, fi_r,
 ):
     sp, tp = sizes
     nz = sp // 2
@@ -200,7 +200,11 @@
     segs = 8
     seg = both // segs
     weights = (w0, w1, w2, w3, w4, w5, w6)
-    count = len(weights)
+    last = len(weights) - 1
+    chunks = [(i, 0, half) for i in range(last)]
+    chunks += [(last, 0, half // 2), (last, half // 2, half // 2)]
+    count = len(chunks)
+    early = 3
     xn = (s + 1 - 2 * x, t)
     core = t + 1 - 2 * lax.rem(t, 2)
     ty = lax.rem(t + 2, tp)
@@ -227,18 +231,27 @@
         pl.semaphore_signal(bar, inc=1, device_id=right, device_id_type=MESH)
 
     own_cols = pl.ds(pl.multiple_of(x * half, half), half)
-    other_cols = pl.ds(pl.multiple_of(xo * half, half), half)
+
+    def weight_cols(p, which):
+        i, off, w = chunks[p]
+        return weights[i].at[:, pl.ds(pl.multiple_of(which * half + off, half // 2), w)]
+
+    def block(p, zz, xx):
+        i, off, w = chunks[p]
+        return wbuf.at[i, zz, xx, :, pl.ds(off, w)]
+
+    def line(p, zz):
+        i, off, w = chunks[p]
+        return wbuf.at[i, zz, :, :, pl.ds(off, w)]
 
     def own_half(p):
-        return pltpu.make_async_copy(
-            weights[p].at[:, own_cols], wbuf.at[p, z, x], wl.at[p]
-        )
+        return pltpu.make_async_copy(weight_cols(p, x), block(p, z, x), wl.at[p])
 
     def swap_half(p):
-        return remote(weights[p].at[:, other_cols], wbuf.at[p, z, x], wx_s.at[p], wx_r.at[p], xn)
+        return remote(weight_cols(p, xo), block(p, z, x), wx_s.at[p], wx_r.at[p], xn)
 
     def swap_half_in(p):
-        return remote(weights[p].at[:, other_cols], wbuf.at[p, z, xo], wx_s.at[p], wx_r.at[p], xn)
+        return remote(weight_cols(p, xo), block(p, z, xo), wx_s.at[p], wx_r.at[p], xn)
 
     x_in = pltpu.make_async_copy(x_hbm, xg.at[x, t], loc.at[2])
     exits = (
@@ -250,7 +263,8 @@
         own_half(p).start()
     pl.semaphore_wait(bar, tp + jnp.where(has_l, 1, 0) + jnp.where(has_r, 1, 0))
 
-    swap_half(0).start()
+    for p in range(early):
+        swap_half(p).start()
     x_moves = {
         0: lambda: remote(x_hbm, xg.at[x, t], xg_s.at[0], xg_r.at[0], xn),
         1: lambda: remote(x_hbm, xg.at[x, t], xg_s.at[1], xg_r.at[1], (s, ty)),
@@ -273,32 +287,45 @@
         x_moves[k]().start()
     pos_out = remote(pos, posn.at[x], po_s, po_r, xn)
     pos_out.start()
-    for p in range(1, count):
+    for p in range(early, count):
         swap_half(p).start()
     for e in exits:
         e.start()
 
-    def z_right(p, d):
-        ref = wbuf.at[p, z - d]
+    def z_right(p, d, part=None):
+        if part is not None:
+            ref = block(p, z, part)
+            return remote(ref, ref, fi_s.at[0], fi_r.at[0], right)
+        ref = block(p, z, x) if (p, d) == (0, 0) else line(p, z - d)
         return remote(ref, ref, zr_s.at[p, d], zr_r.at[p, d], right)
 
-    def z_left(p, d):
-        ref = wbuf.at[p, z + d]
+    def z_left(p, d, part=None):
+        if part is not None:
+            ref = block(p, z, part)
+            return remote(ref, ref, fi_s.at[1], fi_r.at[1], left)
+        ref = block(p, z, x) if (p, d) == (0, 0) else line(p, z + d)
         return remote(ref, ref, zl_s.at[p, d], zl_r.at[p, d], left)
 
     def from_left(p, d):
-        ref = wbuf.at[p, z - 1 - d]
-        return remote(ref, ref, zr_s.at[p, d], zr_r.at[p, d], right)
+        ref = block(p, z - 1, x) if (p, d) == (0, 0) else line(p, z - 1 - d)
+        remote(ref, ref, zr_s.at[p, d], zr_r.at[p, d], right).wait_recv()
+        if (p, d) == (0, 0):
+            ref = block(p, z - 1, xo)
+            remote(ref, ref, fi_s.at[0], fi_r.at[0], right).wait_recv()
 
     def from_right(p, d):
-        ref = wbuf.at[p, z + 1 + d]
-        return remote(ref, ref, zl_s.at[p, d], zl_r.at[p, d], left)
+        ref = block(p, z + 1, x) if (p, d) == (0, 0) else line(p, z + 1 + d)
+        remote(ref, ref, zl_s.at[p, d], zl_r.at[p, d], left).wait_recv()
+        if (p, d) == (0, 0):
+            ref = block(p, z + 1, xo)
+            remote(ref, ref, fi_s.at[1], fi_r.at[1], left).wait_recv()
 
     def issue_own(p):
         if p >= count:
             return
         own_half(p).wait()
-        swap_half_in(p).wait_recv()
+        if p > 0:
+            swap_half_in(p).wait_recv()
 
         @pl.when(has_r)
         def _():
@@ -307,6 +334,18 @@
         @pl.when(has_l)
         def _():
             z_left(p, 0).start()
+
+        if p > 0:
+            return
+        swap_half_in(p).wait_recv()
+
+        @pl.when(has_r)
+        def _():
+            z_right(p, 0, xo).start()
+
+        @pl.when(has_l)
+        def _():
+            z_left(p, 0, xo).start()
 
     relayed = set()
 
@@ -317,7 +356,7 @@
 
         @pl.when(z - 1 - d >= 0)
         def _():
-            from_left(p, d).wait_recv()
+            from_left(p, d)
             if d + 1 < nz - 1:
                 @pl.when(has_r)
                 def _():
@@ -325,7 +364,7 @@
 
         @pl.when(z + 1 + d < nz)
         def _():
-            from_right(p, d).wait_recv()
+            from_right(p, d)
             if d + 1 < nz - 1:
                 @pl.when(has_l)
                 def _():
@@ -344,30 +383,32 @@
 
     issue_own(0)
     issue_own(1)
+    issue_own(2)
     sq[...] = jnp.zeros_like(sq)
     x_in.wait()
     scale_block(x, t)
     relay(0, 0)
-    issue_own(2)
     x_arrive(2)
     scale_block(x, core)
+    x_arrive(1)
+    x_moves[5]().start()
+    scale_block(x, ty)
+    relay(0, 1)
     x_arrive(0)
     x_moves[3]().start()
     x_moves[4]().start()
-    x_arrive(1)
-    x_moves[5]().start()
-    relay(0, 1)
     scale_block(xo, t)
-    scale_block(x, ty)
+    x_arrive(5)
+    scale_block(x, tyc)
+    relay(0, 2)
+    relay(1, 0)
+    x_arrive(4)
+    scale_block(xo, core)
+    relay(1, 1)
+    issue_own(3)
     x_arrive(3)
     x_moves[6]().start()
-    relay(0, 2)
     scale_block(xo, ty)
-    x_arrive(4)
-    scale_block(xo, core)
-    x_arrive(5)
-    scale_block(x, tyc)
-    relay(1, 0)
     x_arrive(6)
     scale_block(xo, tyc)
     total = jnp.sum(sq[...], axis=1, keepdims=True)
@@ -377,6 +418,7 @@
 
     def project(p, use):
         per = krows * 2
+        n, off, width = chunks[p]
 
         def step(i, _):
             at = pl.ds(pl.multiple_of(i * tile, tile), tile)
@@ -387,11 +429,13 @@
                     for xx in range(2):
                         k0 = zz * per + xx * krows - b * feats
                         term = jnp.dot(
-                            lhs[:, k0 : k0 + krows], wbuf[p, zz, xx], preferred_element_type=F32
+                            lhs[:, k0 : k0 + krows],
+                            wbuf[n, zz, xx, :, off : off + width],
+                            preferred_element_type=F32,
                         )
                         acc = term if acc is None else acc + term
             wide = inv[at, :]
-            scale = jnp.concatenate([wide] * (half // 128), axis=1)
+            scale = jnp.concatenate([wide] * (width // 128), axis=1)
             use(at, i, (acc * scale).astype(BF16))
             return 0
 
@@ -417,27 +461,42 @@
     def carry_copy():
         return remote(carry_out, carry_in, ed_s.at[2], ed_r.at[2], right)
 
+    def swap_part(k):
+        if k < 3:
+            return k, slice(0, half)
+        return 3, slice((k - 3) * (half // 2), (k - 2) * (half // 2))
+
     def swap(k):
         at = pl.ds(pl.multiple_of(xo * rows, rows), rows)
-        return remote(mix.at[k, at], got.at[k, x], xe_s.at[k], xe_r.at[k], xn)
+        m, cols = swap_part(k)
+        return remote(
+            mix.at[m, at, cols], got.at[m, x, :, cols], xe_s.at[k], xe_r.at[k], xn
+        )
 
     def swap_start(k):
         swap(k).start()
+        m, cols = swap_part(k)
         at = pl.ds(pl.multiple_of(x * rows, rows), rows)
-        got[k, x] = mix[k, at, :]
+        got[m, x, :, cols] = mix[m, at, cols]
 
     def swap_wait(k):
-        remote(mix.at[k, pl.ds(0, rows)], got.at[k, xo], xe_s.at[k], xe_r.at[k], xn).wait_recv()
+        m, cols = swap_part(k)
+        remote(
+            mix.at[m, pl.ds(0, rows), cols], got.at[m, xo, :, cols], xe_s.at[k], xe_r.at[k], xn
+        ).wait_recv()
+
+    homes = (t, core, ty, tyc)
 
     def exchange(e, j):
-        peer = lax.rem(t + j, tp)
+        peer = homes[2] if j == 2 else homes[1]
         return remote(parts.at[e, j], rbuf.at[e, j], rs_s.at[e, j], rs_r.at[e, j], (s, peer))
 
     def exit_matmul(e):
         exits[e].wait()
-        for j in list(range(1, tp)) + [0]:
-            peer = lax.rem(t + j, tp)
-            cols = pl.ds(pl.multiple_of(peer * feats, feats), feats)
+        for j in (3, 1, 0, 2):
+            cols = pl.ds(pl.multiple_of(homes[j] * feats, feats), feats)
+            if j == 2:
+                exchange(e, 3).wait_recv()
 
             def step(i, _):
                 at = pl.ds(pl.multiple_of(i * tile, tile), tile)
@@ -446,6 +505,8 @@
                 ) + jnp.dot(
                     got[e, 1, at, :], ebuf[e, half : 2 * half, cols], preferred_element_type=F32
                 )
+                if j == 2:
+                    acc = acc + rbuf[e, 3, at, :].astype(F32)
                 parts[e, j, at, :] = acc.astype(BF16)
                 return 0
 
@@ -454,10 +515,9 @@
                 exchange(e, j).start()
 
     def exit_sum(e):
-        for j in range(1, tp):
+        total = parts[e, 0].astype(F32)
+        for j in (1, 2):
             exchange(e, j).wait_recv()
-        total = parts[e, 0].astype(F32)
-        for j in range(1, tp):
             total = total + rbuf[e, j].astype(F32)
         sums[e] = total
 
@@ -466,7 +526,6 @@
             relay(p, d)
         issue_own(p + 3)
 
-    issue_own(3)
 
     def keep_lru(at, i, value):
         lbuf[pl.ds(pl.multiple_of(8 + i * tile, 8), tile), :] = value.astype(F32)
@@ -600,38 +659,54 @@
             conv = term if conv is None else conv + term
         mix[1, pl.ds(i * tile, tile), :] = (lbuf[pl.ds(8 + i * tile, tile), :] * conv).astype(BF16)
     swap_start(1)
-    relay(5, 0)
-    relay(5, 1)
     swap_wait(1)
     exit_matmul(1)
-    for d in range(2, nz - 1):
+    for d in range(nz - 1):
         relay(5, d)
 
     def keep_mix(k):
+        m, cols = swap_part(k)
+
         def use(at, i, value):
-            mix[k, at, :] = value
+            mix[m, at, cols] = value
         return use
+
+    def merge(part):
+        for xx in range(2):
+            here = slice(part * (half // 2), (part + 1) * (half // 2))
+            start = xx * half + part * (half // 2)
+            cols = slice(start, start + half // 2)
+            out[:, cols] = (
+                jax.nn.sigmoid(got[2, xx, :, here].astype(F32)) * sums[1, :, cols]
+                + jax.nn.sigmoid(got[3, xx, :, here].astype(F32)) * sums[0, :, cols]
+            ).astype(BF16)
 
     project(5, keep_mix(2))
     swap_start(2)
     exit_sum(0)
-    for d in range(nz - 1):
-        relay(6, d)
-    project(6, keep_mix(3))
-    swap_start(3)
+    for p in (6, 7):
+        for d in range(nz - 1):
+            relay(p, d)
+        project(p, keep_mix(p - 3))
+        swap_start(p - 3)
     exit_sum(1)
     swap_wait(2)
-    swap_wait(3)
-    for xx in range(2):
-        cols = slice(xx * half, (xx + 1) * half)
-        out[:, cols] = (
-            jax.nn.sigmoid(got[2, xx].astype(F32)) * sums[1, :, cols]
-            + jax.nn.sigmoid(got[3, xx].astype(F32)) * sums[0, :, cols]
-        ).astype(BF16)
+    for part in range(2):
+        swap_wait(3 + part)
+        merge(part)
 
     pos_out.wait_send()
     for p in range(count):
         swap_half(p).wait_send()
+        if p == 0:
+            @pl.when(has_r)
+            def _():
+                z_right(0, 0, xo).wait_send()
+
+            @pl.when(has_l)
+            def _():
+                z_left(0, 0, xo).wait_send()
+
         for d in range(nz - 1):
             @pl.when(has_r & (z - d >= 0))
             def _():
@@ -648,7 +723,7 @@
         edge(sbuf, 1).wait_send()
         carry_copy().wait_send()
 
-    for k in range(4):
+    for k in range(5):
         swap(k).wait_send()
     for e in range(2):
         for j in range(1, tp):
@@ -697,10 +772,10 @@
             pltpu.VMEM((2, tp, rows, feats), BF16),
             pltpu.VMEM((2, rows, width), F32),
             pltpu.VMEM((2,) + ec.shape, BF16),
-            dma((7,)), dma((7,)), dma((7,)),
-            dma((7, nz - 1)), dma((7, nz - 1)), dma((7, nz - 1)), dma((7, nz - 1)),
+            dma((8,)), dma((8,)), dma((8,)),
+            dma((8, nz - 1)), dma((8, nz - 1)), dma((8, nz - 1)), dma((8, nz - 1)),
             dma((7,)), dma((7,)), dma, dma, dma((3,)), dma((3,)),
-            dma((4,)), dma((4,)), dma((2, tp)), dma((2, tp)), dma((3,)),
+            dma((5,)), dma((5,)), dma((2, tp)), dma((2, tp)), dma((3,)), dma((2,)), dma((2,)),
         ],
         compiler_params=pltpu.CompilerParams(
             collective_id=0, has_side_effects=True, vmem_limit_bytes=62 * 1024 * 1024

time: 155 us -> 149 us (0.961)
  Pallas kernels: 151 us -> 146 us
    pallas_call x1, Pallas kernels: 151 us -> 146 us  [paired(): kernel(x, gain.reshape(tp, 1, feats), win, wgate, wc, wx, wb, mconv, mlru...]
where the time goes in v2:
time: 149 us
  Pallas kernels  146 us (98%)
  local copies, waits for them, and re-layouts  1.95 us (1%)
    pallas_call x1, Pallas kernels, paired(): kernel(x, gain.reshape(tp, 1, feats), win, wgate, wc, wx, wb, mconv, mlru...  146 us

profile of v2, /device:TPU:0, one launch (start us, length us, event | category | flops | bytes accessed | tf_op | source)
XLA Modules:
  0.0 149.3 jit_solution(1673532815863855145)
XLA Ops:
  0.0 0.1 pad.2.clone
  0.1 1.4 maximum_maximum_fusion.pos
  1.5 145.9 %shard_map.181 = bf16[512,512]{1,0:T(8,128)(2,1)} custom-call(bf16[512,512]{1,0:T(8,128)(2,1)} %x_hbm.1, f32[4,1,512]{2,1,0:T(1,128)} %bitcast.5, bf16[256,512]{1,0:T(8,128)(2,1)} %w0.1, bf16[256,512]{1,0:T(8,128)(2,1)} %w1.1, bf16[256,512]{1,0:T(8,128)(2,1)} %w2.1, bf16[256,512]{1,0:T(8,128)(2,1)} %w3.1, bf16[256,512]{1,0:T(8,128)(2,1)} %w4.1, ...), custom_call_target="tpu_custom_call" | custom-call | tf_op jit(solution)/shard_map/pallas_call | solution.py:784
  147.4 1.9 %copy.21 = bf16[512,512]{1,0:T(8,128)(2,1)} copy(bf16[512,512]{1,0:T(8,128)(2,1)} %shard_map.181) | data formatting | bytes 1048576
  (1 shorter events, 0.0 us)
